TPU v7x, 32 devices: a whole 2x2x4 slice. The times are simulated.
32 devices in a mesh: ep: 8 (over z, core), tp: 4 (over y, x).
Axes of the slice: x: 2, y: 2, z: 4, core: 2. Of those that a mesh axis runs over, the one named last changes fastest.
Arguments:
- tokens: bfloat16 [2048, 2048], P('ep'), may hold values from -6 to 6
- gate_proj: bfloat16 [8, 2048, 4096], P('ep', None, 'tp'), may hold values from -0.125 to 0.125
- up_proj: bfloat16 [8, 2048, 4096], P('ep', None, 'tp'), may hold values from -0.125 to 0.125
- down_proj: bfloat16 [8, 4096, 2048], P('ep', 'tp'), may hold values from -0.09375 to 0.09375
- side_input_weight: bfloat16 [2048, 1024], P(None, 'tp'), may hold values from -0.125 to 0.125
- dense_out: bfloat16 [1024, 2048], P(None, 'tp'), may hold values from -0.1875 to 0.1875
- dense_gate: bfloat16 [2048], replicated, may hold values from -0.125 to 0.125
- chosen_rows: int32 [8, 256], P(None, 'ep'), may hold values from 0 to 255, as said below
- choice_weights: float32 [8, 256], P(None, 'ep'), may hold values from 0.25 to 1
Outputs:
- mixed: bfloat16 [2048, 2048], P('ep', 'tp')
Inputs may be any that keep to these rules, and one draw needn't show every extreme that they name: `chosen_rows`: for each expert and each block of 32 columns (one index of ep), the 32 rows are distinct rows of that index's 256 tokens; every expert reads exactly 32 tokens of every index.
All inputs are finite; a program needn't handle non-finite values.
Results may differ from a plain program's by a relative error of at most 0.015.
Values may be sent and summed in bfloat16 or wider, within the bound.
A program may use at most 64 MiB of HBM per device.

v0:
```python
import functools

import jax
import jax.numpy as jnp
from jax import lax
from jax.experimental import pallas as pl
from jax.experimental.pallas import tpu as pltpu
from jax.sharding import PartitionSpec as P

MESH = pl.DeviceIdType.MESH
LANES = 128


def plain_per_device(
    tokens,
    gate_proj,
    up_proj,
    down_proj,
    side_input_weight,
    dense_out,
    dense_gate,
    chosen_rows,
    choice_weights,
):
    tok_rows = tokens.shape[0]
    width = tokens.shape[1] // lax.axis_size("tp")
    column_position = lax.axis_index("tp") * width
    own_cols = lax.dynamic_slice_in_dim(tokens, column_position, width, 1)
    expert_count, slot_rows = chosen_rows.shape
    capacity = expert_count * slot_rows
    picked = jnp.take(own_cols, chosen_rows.reshape(-1), axis=0).reshape(
        expert_count, slot_rows, width
    )
    arrived = lax.all_to_all(picked, "ep", split_axis=0, concat_axis=1, tiled=True).reshape(
        capacity, width
    )
    piece = lax.all_gather(arrived, "tp", axis=1, tiled=True)
    gate_val = jnp.dot(piece, gate_proj[0], preferred_element_type=jnp.float32)
    up_val = jnp.dot(piece, up_proj[0], preferred_element_type=jnp.float32)
    hidden = (jax.nn.silu(gate_val) * up_val).astype(jnp.bfloat16)
    summed = lax.psum_scatter(
        lax.dot_general(
            down_proj[0], hidden, (((0,), (1,)), ((), ())), preferred_element_type=jnp.float32
        ).astype(jnp.bfloat16),
        "tp",
        scatter_dimension=0,
        tiled=True,
    )
    returned = lax.all_to_all(summed, "ep", split_axis=1, concat_axis=1, tiled=True)
    hits = (
        chosen_rows.reshape(-1)[:, None] == jnp.arange(tok_rows, dtype=jnp.int32)[None, :]
    ).astype(jnp.bfloat16)
    scaled = returned.astype(jnp.float32) * choice_weights.reshape(-1)[None, :]
    high_part = scaled.astype(jnp.bfloat16)
    lower_half = (scaled - high_part.astype(jnp.float32)).astype(jnp.bfloat16)
    contract = (((0,), (1,)), ((), ()))
    routed = lax.dot_general(
        hits, high_part, contract, preferred_element_type=jnp.float32
    ) + lax.dot_general(hits, lower_half, contract, preferred_element_type=jnp.float32)
    dense_hidden = jax.nn.silu(
        jnp.dot(tokens, side_input_weight, preferred_element_type=jnp.float32)
    ).astype(jnp.bfloat16)
    dense_val = jnp.dot(
        lax.all_gather(dense_hidden, "tp", axis=1, tiled=True),
        dense_out,
        preferred_element_type=jnp.float32,
    )
    side_gate = jax.nn.sigmoid(jnp.dot(tokens, dense_gate, preferred_element_type=jnp.float32))
    return (routed + side_gate[:, None] * dense_val).astype(jnp.bfloat16)


def dot(a, b):
    return jnp.dot(a, b, preferred_element_type=jnp.float32)


def silu(v):
    return v / (1.0 + jnp.exp(-v))


def layer_kernel(
    n_ep,
    slot,
    tok_hbm,
    gate_hbm,
    up_hbm,
    down_hbm,
    side_hbm,
    dout_hbm,
    dgate_ref,
    rows_ref,
    cw_ref,
    out_ref,
    tok,
    w_gate,
    w_up,
    w_down,
    w_side,
    w_dout,
    pick,
    xin,
    g_acc,
    u_acc,
    hid,
    comb,
    dhid,
    part,
    d_in,
    rx,
    ry,
    pair,
    fin,
    back,
    load_sem,
    send_sem,
    z_sem,
    ag_sem,
    dh_sem,
    rsd_sem,
    rsx_sem,
    rsy_sem,
    ret_sem,
):
    e = lax.axis_index("ep")
    p = lax.axis_index("tp")
    px = p + 1 - 2 * (p % 2)
    py = p + 2 - 4 * (p // 2)
    pd = px + 2 - 4 * (px // 2)
    z = e // 2
    nz = n_ep // 2
    width = xin.shape[2]
    tok_rows = tok.shape[0]
    side = w_side.shape[1]
    to_x, to_y = {"tp": px}, {"tp": py}

    loads = []
    for i, (src, dst) in enumerate(
        (
            (tok_hbm, tok),
            (side_hbm, w_side),
            (gate_hbm.at[0], w_gate),
            (up_hbm.at[0], w_up),
            (down_hbm.at[0], w_down),
            (dout_hbm, w_dout),
        )
    ):
        copy = pltpu.make_async_copy(src, dst, load_sem.at[i])
        copy.start()
        loads.append(copy)

    barrier = pltpu.get_barrier_semaphore()
    for k in range(1, n_ep):
        pl.semaphore_signal(
            barrier, inc=1, device_id={"ep": (e + k) % n_ep}, device_id_type=MESH
        )
    for there in (to_x, to_y):
        pl.semaphore_signal(barrier, inc=1, device_id=there, device_id_type=MESH)

    def block(owner):
        return pl.ds(pl.multiple_of(owner * slot, slot), slot)

    sends = []

    def send(src, dst, sem, there):
        copy = pltpu.make_async_remote_copy(
            src_ref=src,
            dst_ref=dst,
            send_sem=send_sem.at[len(sends)],
            recv_sem=sem,
            device_id=there,
            device_id_type=MESH,
        )
        copy.start()
        sends.append(copy)

    def arrive(dst, sem):
        pltpu.make_async_remote_copy(
            src_ref=dst,
            dst_ref=dst,
            send_sem=send_sem.at[0],
            recv_sem=sem,
            device_id=to_x,
            device_id_type=MESH,
        ).wait_recv()

    rows_t = rows_ref[...].astype(jnp.float32).T
    cw_t = cw_ref[...].T
    lane = lax.broadcasted_iota(jnp.int32, (slot, tok_rows), 1).astype(jnp.float32)
    hits = jnp.concatenate(
        [jnp.where(rows_t[:, k : k + 1] == lane, 1.0, 0.0) for k in range(n_ep)], axis=0
    )
    loads[0].wait()
    own = pl.ds(pl.multiple_of(p * width, width), width)
    pick[...] = dot(hits.astype(jnp.bfloat16), tok[:, own]).astype(jnp.bfloat16)
    pl.semaphore_wait(barrier, n_ep + 1)

    if nz == 4:
        upper = z // 2
        inner = (z + upper) % 2
        chips = [z, z + 1 - 2 * (z % 2), 2 - upper, 3 - 3 * upper]
        goals = chips
        places = [0, 1, 3 - inner, 3 - inner]
        turn = [2, 3, 1, 0]
    else:
        chips = [(z + nz - g) % nz for g in range(nz)]
        goals = [(z + g) % nz for g in range(nz)]
        places = list(range(nz))
        turn = [*range(1, nz), 0]
    core = e % 2
    partner = e + 1 - 2 * core

    def at(pos):
        return pl.ds(pl.multiple_of(pos * slot, slot), slot)

    send(pick.at[block(partner)], xin.at[p, at(1)], z_sem.at[1], {"ep": partner})
    for g in range(1, nz):
        for c in range(2):
            peer = 2 * goals[g] + c
            mine = 2 * places[g] + core
            send(pick.at[block(peer)], xin.at[p, at(mine)], z_sem.at[mine], {"ep": peer})
    xin[p, at(0)] = pick[block(e), :]

    def spread(pos):
        ref = xin.at[p, at(pos)]
        send(ref, ref, ag_sem.at[0, pos], to_x)
        send(ref, ref, ag_sem.at[1, pos], to_y)

    def forward(pos):
        if pos % 2 == 0:
            ref = xin.at[px, at(pos)]
            arrive(ref, ag_sem.at[0, pos])
            send(ref, ref, ag_sem.at[2, pos], to_y)
        else:
            ref = xin.at[py, at(pos)]
            arrive(ref, ag_sem.at[1, pos])
            send(ref, ref, ag_sem.at[2, pos], to_x)

    spread(0)
    loads[1].wait()
    dhid[p] = silu(dot(tok[...], w_side[...])).astype(jnp.bfloat16)
    arrive(xin.at[p, at(1)], z_sem.at[1])
    spread(1)
    send(dhid.at[p], dhid.at[p], dh_sem.at[0], to_x)
    send(dhid.at[p], dhid.at[p], dh_sem.at[1], to_y)

    weight = jnp.concatenate([cw_t[:, k : k + 1] for k in range(n_ep)], axis=0)
    both = (hits * weight).T
    high = both.astype(jnp.bfloat16)
    comb[0] = high
    comb[1] = (both - high.astype(jnp.float32)).astype(jnp.bfloat16)

    tile = 2 * LANES
    n_tiles = g_acc.shape[1] // tile
    f32 = jnp.float32
    half = tok_rows // 2

    def gate_up(q, first):
        rows = pl.ds(pl.multiple_of(q * width, width), width)

        @pl.loop(0, n_tiles)
        def _(n):
            cols = pl.ds(pl.multiple_of(n * tile, tile), tile)
            g = dot(xin[q], w_gate[rows, cols])
            u = dot(xin[q], w_up[rows, cols])
            if first:
                g_acc[:, cols] = g
                u_acc[:, cols] = u
            else:
                g_acc[:, cols] += g
                u_acc[:, cols] += u

    def gate_up_last(q):
        rows = pl.ds(pl.multiple_of(q * width, width), width)

        @pl.loop(0, n_tiles)
        def _(n):
            cols = pl.ds(pl.multiple_of(n * tile, tile), tile)
            g = g_acc[:, cols] + dot(xin[q], w_gate[rows, cols])
            u = u_acc[:, cols] + dot(xin[q], w_up[rows, cols])
            hid[:, cols] = (silu(g) * u).astype(jnp.bfloat16)

    def down(to, q):

        @pl.loop(0, width // tile)
        def _(n):
            cols = pl.ds(pl.multiple_of(n * tile, tile), tile)
            src = pl.ds(pl.multiple_of(q * width + n * tile, tile), tile)
            part[to, :, cols] = dot(hid[...], w_down[:, src]).astype(jnp.bfloat16)

    def wait_x():
        for pos in range(n_ep):
            if pos % 2:
                arrive(xin.at[px, at(pos)], ag_sem.at[0, pos])

    def wait_y():
        for pos in range(n_ep):
            if pos % 2 == 0:
                arrive(xin.at[py, at(pos)], ag_sem.at[1, pos])

    def wait_d():
        for pos in range(n_ep):
            arrive(xin.at[pd, at(pos)], ag_sem.at[2, pos])

    def first_d(g):
        even, odd = at(2 * g), at(2 * g + 1)
        send(part.at[3, odd], d_in.at[odd], rsd_sem.at[2 * g + 1], to_x)
        send(part.at[3, even], d_in.at[even], rsd_sem.at[2 * g], to_y)

    def direct_x(g):
        odd = at(2 * g + 1)
        send(part.at[1, odd], rx.at[odd], rsx_sem.at[2 * g + 1], to_x)

    def direct_y(g):
        even = at(2 * g)
        send(part.at[2, even], ry.at[even], rsy_sem.at[2 * g], to_y)

    def joined(g):
        for pos, src, dst, sem, there in (
            (2 * g, 1, rx, rsx_sem, to_x),
            (2 * g + 1, 2, ry, rsy_sem, to_y),
        ):
            b = at(pos)
            arrive(d_in.at[b], rsd_sem.at[pos])
            pair[b, :] = (part[src, b, :].astype(f32) + d_in[b, :].astype(f32)).astype(
                jnp.bfloat16
            )
            send(pair.at[b], dst.at[b], sem.at[pos], there)

    def finish(g):
        for c in range(2):
            pos = 2 * g + c
            b = at(pos)
            arrive(rx.at[b], rsx_sem.at[pos])
            arrive(ry.at[b], rsy_sem.at[pos])
            total = (
                part[0, b, :].astype(f32) + rx[b, :].astype(f32) + ry[b, :].astype(f32)
            ).astype(jnp.bfloat16)
            if pos == 0:
                back[block(e), :] = total
            else:
                fin[b, :] = total
                owner = partner if g == 0 else 2 * chips[g] + c
                send(fin.at[b], back.at[block(e)], ret_sem.at[e], {"ep": owner})

    lag = n_ep
    for pos in range(2, n_ep):
        arrive(xin.at[p, at(pos)], z_sem.at[pos])
        spread(pos)
        if pos >= lag:
            forward(pos - lag)
    loads[2].wait()
    loads[3].wait()
    gate_up(p, True)
    for pos in range(n_ep - lag, n_ep):
        forward(pos)
    arrive(dhid.at[px], dh_sem.at[0])
    ref = dhid.at[px, pl.ds(0, half)]
    send(ref, ref, dh_sem.at[2], to_y)
    arrive(dhid.at[py], dh_sem.at[1])
    ref = dhid.at[py, pl.ds(half, half)]
    send(ref, ref, dh_sem.at[3], to_x)
    wait_x()
    gate_up(px, False)
    wait_y()
    gate_up(py, False)
    wait_d()
    gate_up_last(pd)

    loads[4].wait()
    down(3, pd)
    first_d(turn[0])
    first_d(turn[1])
    down(1, px)
    direct_x(turn[0])
    down(2, py)
    direct_y(turn[0])
    direct_x(turn[1])
    direct_y(turn[1])
    down(0, p)
    for i in range(nz):
        joined(turn[i])
        if i + 2 < nz:
            first_d(turn[i + 2])
            direct_x(turn[i + 2])
            direct_y(turn[i + 2])
        if i >= 1:
            finish(turn[i - 1])
        if i == 1:
            arrive(dhid.at[pd, pl.ds(0, half)], dh_sem.at[2])
            arrive(dhid.at[pd, pl.ds(half, half)], dh_sem.at[3])
            loads[5].wait()
            total = dot(dhid[0], w_dout[pl.ds(0, side)])
            for q in range(1, dhid.shape[0]):
                total += dot(dhid[q], w_dout[pl.ds(q * side, side)])
            logit = jnp.sum(
                tok[...].astype(f32) * dgate_ref[...].reshape(1, tok.shape[1]).astype(f32),
                axis=1,
                keepdims=True,
            )
            g_acc[:, pl.ds(0, width)] = total / (1.0 + jnp.exp(-logit))
    finish(turn[-1])

    for k in range(1, n_ep):
        owner = (e + n_ep - k) % n_ep
        arrive(back.at[block(owner)], ret_sem.at[owner])
    out_ref[...] = (
        g_acc[:, pl.ds(0, width)] + dot(comb[0], back[...]) + dot(comb[1], back[...])
    )
    for copy in sends:
        copy.wait_send()


def fused_per_device(
    tokens,
    gate_proj,
    up_proj,
    down_proj,
    side_input_weight,
    dense_out,
    dense_gate,
    chosen_rows,
    choice_weights,
):
    n_ep, slot = chosen_rows.shape
    n_tp = lax.axis_size("tp")
    tok_rows, d = tokens.shape
    width = d // n_tp
    ff = gate_proj.shape[2]
    side = side_input_weight.shape[1]
    cap = n_ep * slot
    bf16, f32 = jnp.bfloat16, jnp.float32
    n_sends = 2 * (n_ep - 1) + 2 * n_ep + n_ep + 4 + 3 * n_ep
    hbm = pl.BlockSpec(memory_space=pltpu.HBM)
    vmem = pl.BlockSpec(memory_space=pltpu.VMEM)
    return pl.pallas_call(
        functools.partial(layer_kernel, n_ep, slot),
        out_shape=pltpu.VMEM((tok_rows, width), f32),
        in_specs=[hbm] * 6 + [vmem] * 3,
        out_specs=vmem,
        scratch_shapes=[
            pltpu.VMEM((tok_rows, d), bf16),
            pltpu.VMEM((d, ff), bf16),
            pltpu.VMEM((d, ff), bf16),
            pltpu.VMEM((ff, d), bf16),
            pltpu.VMEM((d, side), bf16),
            pltpu.VMEM((n_tp * side, width), bf16),
            pltpu.VMEM((cap, width), bf16),
            pltpu.VMEM((n_tp, cap, width), bf16),
            pltpu.VMEM((cap, ff), f32),
            pltpu.VMEM((cap, ff), f32),
            pltpu.VMEM((cap, ff), bf16),
            pltpu.VMEM((2, tok_rows, cap), bf16),
            pltpu.VMEM((n_tp, tok_rows, side), bf16),
            pltpu.VMEM((4, cap, width), bf16),
            pltpu.VMEM((cap, width), bf16),
            pltpu.VMEM((cap, width), bf16),
            pltpu.VMEM((cap, width), bf16),
            pltpu.VMEM((cap, width), bf16),
            pltpu.VMEM((cap, width), bf16),
            pltpu.VMEM((cap, width), bf16),
            pltpu.SemaphoreType.DMA((6,)),
            pltpu.SemaphoreType.DMA((n_sends,)),
            pltpu.SemaphoreType.DMA((n_ep,)),
            pltpu.SemaphoreType.DMA((3, n_ep)),
            pltpu.SemaphoreType.DMA((4,)),
            pltpu.SemaphoreType.DMA((n_ep,)),
            pltpu.SemaphoreType.DMA((n_ep,)),
            pltpu.SemaphoreType.DMA((n_ep,)),
            pltpu.SemaphoreType.DMA((n_ep,)),
        ],
        compiler_params=pltpu.CompilerParams(collective_id=0, has_side_effects=True),
    )(
        tokens,
        gate_proj,
        up_proj,
        down_proj,
        side_input_weight,
        dense_out,
        dense_gate,
        chosen_rows,
        choice_weights,
    ).astype(bf16)


def per_device(*args):
    tokens, gate_proj, chosen_rows = args[0], args[1], args[7]
    n_ep, slot = chosen_rows.shape
    n_tp = lax.axis_size("tp")
    width, tile = tokens.shape[1] // n_tp, 2 * LANES
    fits = (
        n_tp == 4
        and n_ep % 4 == 0
        and tokens.shape[0] == n_ep * slot
        and slot % 16 == 0
        and width % tile == 0
        and gate_proj.shape[2] % tile == 0
        and args[4].shape[1] % LANES == 0
    )
    return fused_per_device(*args) if fits else plain_per_device(*args)


def solution(mesh):
    placed = (
        P("ep", None),
        P("ep", None, "tp"),
        P("ep", None, "tp"),
        P("ep", "tp", None),
        P(None, "tp"),
        P(None, "tp"),
        P(),
        P(None, "ep"),
        P(None, "ep"),
    )
    return jax.shard_map(
        per_device, mesh=mesh, in_specs=placed, out_specs=P("ep", "tp"), check_vma=False
    )
```

profile of v0, /device:TPU:0, one launch (start us, length us, event | category | flops | bytes accessed | tf_op | source)
XLA Modules:
  0.0 38.6 jit_solution(8225858460797818516)
XLA Ops:
  0.0 37.9 %shard_map.91 = f32[256,512]{1,0:T(8,128)S(1)} custom-call(bf16[256,2048]{1,0:T(8,128)(2,1)} %tok_hbm.1, bf16[1,2048,1024]{2,1,0:T(8,128)(2,1)} %gate_hbm.1, bf16[1,2048,1024]{2,1,0:T(8,128)(2,1)} %up_hbm.1, bf16[1,1024,2048]{2,1,0:T(8,128)(2,1)} %down_hbm.1, bf16[2048,256]{1,0:T(8,128)(2,1)} %side_hbm.1, bf16[1024,512]{1,0:T(8,128)(2,1)} %dout_hbm.1, ...), custom_call_target="tpu_custom_call" | custom-call | tf_op jit(solution)/shard_map/pallas_call | solution.py:434
  37.9 0.7 %convert_element_type.3 = bf16[256,512]{1,0:T(8,128)(2,1)} convert(f32[256,512]{1,0:T(8,128)S(1)} %shard_map.91) | non-fusion elementwise | flops 131072 | bytes 786432 | tf_op jit(solution)/shard_map/convert_element_type | solution.py:481
where the time goes:
time: 38.8 us; the launch traced here: 38.6 us
  Pallas kernels  37.9 us (98%)
  other arithmetic  0.74 us (2%)
    pallas_call x1, Pallas kernels, fused_per_device(): pl.pallas_call(functools.partial(layer_kernel, n_ep, slot), out_shape=plt...  37.9 us

commit v1 on v0

v1 whole, which is shorter than its diff:
```python
import functools

import jax
import jax.numpy as jnp
from jax import lax
from jax.experimental import pallas as pl
from jax.experimental.pallas import tpu as pltpu
from jax.sharding import PartitionSpec as P

MESH = pl.DeviceIdType.MESH
LANES = 128


def plain_per_device(
    tokens,
    gate_proj,
    up_proj,
    down_proj,
    side_input_weight,
    dense_out,
    dense_gate,
    chosen_rows,
    choice_weights,
):
    tok_rows = tokens.shape[0]
    width = tokens.shape[1] // lax.axis_size("tp")
    column_position = lax.axis_index("tp") * width
    own_cols = lax.dynamic_slice_in_dim(tokens, column_position, width, 1)
    expert_count, slot_rows = chosen_rows.shape
    capacity = expert_count * slot_rows
    picked = jnp.take(own_cols, chosen_rows.reshape(-1), axis=0).reshape(
        expert_count, slot_rows, width
    )
    arrived = lax.all_to_all(picked, "ep", split_axis=0, concat_axis=1, tiled=True).reshape(
        capacity, width
    )
    piece = lax.all_gather(arrived, "tp", axis=1, tiled=True)
    gate_val = jnp.dot(piece, gate_proj[0], preferred_element_type=jnp.float32)
    up_val = jnp.dot(piece, up_proj[0], preferred_element_type=jnp.float32)
    hidden = (jax.nn.silu(gate_val) * up_val).astype(jnp.bfloat16)
    summed = lax.psum_scatter(
        lax.dot_general(
            down_proj[0], hidden, (((0,), (1,)), ((), ())), preferred_element_type=jnp.float32
        ).astype(jnp.bfloat16),
        "tp",
        scatter_dimension=0,
        tiled=True,
    )
    returned = lax.all_to_all(summed, "ep", split_axis=1, concat_axis=1, tiled=True)
    hits = (
        chosen_rows.reshape(-1)[:, None] == jnp.arange(tok_rows, dtype=jnp.int32)[None, :]
    ).astype(jnp.bfloat16)
    scaled = returned.astype(jnp.float32) * choice_weights.reshape(-1)[None, :]
    high_part = scaled.astype(jnp.bfloat16)
    lower_half = (scaled - high_part.astype(jnp.float32)).astype(jnp.bfloat16)
    contract = (((0,), (1,)), ((), ()))
    routed = lax.dot_general(
        hits, high_part, contract, preferred_element_type=jnp.float32
    ) + lax.dot_general(hits, lower_half, contract, preferred_element_type=jnp.float32)
    dense_hidden = jax.nn.silu(
        jnp.dot(tokens, side_input_weight, preferred_element_type=jnp.float32)
    ).astype(jnp.bfloat16)
    dense_val = jnp.dot(
        lax.all_gather(dense_hidden, "tp", axis=1, tiled=True),
        dense_out,
        preferred_element_type=jnp.float32,
    )
    side_gate = jax.nn.sigmoid(jnp.dot(tokens, dense_gate, preferred_element_type=jnp.float32))
    return (routed + side_gate[:, None] * dense_val).astype(jnp.bfloat16)


def dot(a, b):
    return jnp.dot(a, b, preferred_element_type=jnp.float32)


def silu(v):
    return v / (1.0 + jnp.exp(-v))


def layer_kernel(
    slot,
    tok_hbm,
    gate_hbm,
    up_hbm,
    down_hbm,
    side_hbm,
    dout_hbm,
    dgate_hbm,
    rows_hbm,
    cw_hbm,
    out_ref,
    dgate_ref,
    rows_ref,
    cw_ref,
    tok,
    w_gate,
    w_up,
    w_down,
    w_side,
    w_dout,
    pick,
    xin,
    g_acc,
    u_acc,
    hid,
    comb,
    dhid,
    dense,
    part,
    d_in,
    rx,
    ry,
    pair,
    fin,
    back,
    load_sem,
    send_sem,
    far_sem,
    z_sem,
    ag_sem,
    dh_sem,
    rsd_sem,
    rsx_sem,
    rsy_sem,
    ret_sem,
):
    n_ep = rows_ref.shape[0]
    e = lax.axis_index("ep")
    p = lax.axis_index("tp")
    px = p + 1 - 2 * (p % 2)
    py = p + 2 - 4 * (p // 2)
    pd = px + 2 - 4 * (px // 2)
    z = e // 2
    core = e % 2
    partner = e + 1 - 2 * core
    upper = z // 2
    inner = (z + upper) % 2
    chips = [z, 3 - 3 * upper, 2 - upper, z + 1 - 2 * (z % 2)]
    width = out_ref.shape[1]
    tok_rows = tok.shape[0]
    side = w_side.shape[1]
    to_x, to_y = {"tp": px}, {"tp": py}
    f32, bf16 = jnp.float32, jnp.bfloat16
    scope = jax.named_scope

    barrier = pltpu.get_barrier_semaphore()
    for k in range(1, n_ep):
        pl.semaphore_signal(
            barrier, inc=1, device_id={"ep": (e + k) % n_ep}, device_id_type=MESH
        )
    for there in (to_x, to_y):
        pl.semaphore_signal(barrier, inc=1, device_id=there, device_id_type=MESH)

    loads = []
    for i, (src, dst) in enumerate(
        (
            (tok_hbm, tok),
            (side_hbm, w_side),
            (gate_hbm.at[0], w_gate),
            (up_hbm.at[0], w_up),
            (down_hbm.at[0], w_down),
            (dout_hbm, w_dout),
            (rows_hbm, rows_ref),
            (cw_hbm, cw_ref),
            (dgate_hbm, dgate_ref),
        )
    ):
        loads.append(pltpu.make_async_copy(src, dst, load_sem.at[i]))
    for i in (6, 0, 1, 7, 8, 2, 3, 4, 5):
        loads[i].start()

    def block(owner):
        return pl.ds(pl.multiple_of(owner * slot, slot), slot)

    def at(pos):
        return pl.ds(pos * slot, slot)

    def cols_of(q):
        return pl.ds(pl.multiple_of(q * width, width), width)

    sends = []

    def send(src, dst, sem, there):
        copy = pltpu.make_async_remote_copy(
            src_ref=src,
            dst_ref=dst,
            send_sem=send_sem.at[len(sends)],
            recv_sem=sem,
            device_id=there,
            device_id_type=MESH,
        )
        copy.start()
        sends.append(copy)

    def arrive(dst, sem):
        pltpu.make_async_remote_copy(
            src_ref=dst,
            dst_ref=dst,
            send_sem=send_sem.at[0],
            recv_sem=sem,
            device_id=to_x,
            device_id_type=MESH,
        ).wait_recv()

    with scope("hits"):
        loads[6].wait()
        rows_t = rows_ref[...].astype(f32).T
        lane = lax.broadcasted_iota(jnp.int32, (slot, tok_rows), 1).astype(f32)
        hits = jnp.concatenate(
            [jnp.where(rows_t[:, k : k + 1] == lane, 1.0, 0.0) for k in range(n_ep)], axis=0
        )
        chosen = hits.astype(bf16)
        loads[0].wait()
    with scope("pick"):
        for q in range(tok.shape[1] // width):
            cols = pl.ds(q * width, width)
            pick[:, cols] = dot(chosen, tok[:, cols]).astype(bf16)
    with scope("barrier"):
        pl.semaphore_wait(barrier, n_ep + 1)

    own, far = cols_of(p), cols_of(pd)

    def slot_of(pos):
        return pl.ds(pl.multiple_of(pos * slot, slot), slot)

    crossing = []
    for i, (g, c) in enumerate(((1, 0), (1, 1), (2, 0), (2, 1))):
        peer = 2 * chips[g] + c
        pos = 2 * (1 + inner) + core
        crossing.append(
            pltpu.make_async_remote_copy(
                src_ref=pick.at[block(peer), own],
                dst_ref=xin.at[slot_of(pos), own],
                send_sem=far_sem.at[i],
                recv_sem=z_sem.at[pos],
                device_id={"ep": peer},
                device_id_type=MESH,
            )
        )

    def far_sends():
        for copy in crossing:
            copy.start()

    pl.when(inner == 0)(far_sends)
    for c in range(2):
        peer = 2 * chips[3] + c
        pos = 6 + core
        send(pick.at[block(peer)], xin.at[slot_of(pos)], z_sem.at[pos], {"ep": peer})
    send(pick.at[block(partner)], xin.at[at(1)], z_sem.at[1], {"ep": partner})
    with scope("dhid"):
        loads[1].wait()
        dhid[p] = silu(dot(tok[...], w_side[...])).astype(bf16)
    send(dhid.at[p], dhid.at[p], dh_sem.at[0], to_x)
    send(dhid.at[p], dhid.at[p], dh_sem.at[1], to_y)
    xin[at(0), :] = pick[block(e), :]

    def combine_weights():
        loads[7].wait()
        cw_t = cw_ref[...].T
        weight = jnp.concatenate([cw_t[:, k : k + 1] for k in range(n_ep)], axis=0)
        both = (hits * weight).T
        high = both.astype(bf16)
        comb[0] = high
        comb[1] = (both - high.astype(f32)).astype(bf16)

    tile = 2 * LANES

    def gate_up_part(g):
        rows = pl.ds(2 * g * slot, 2 * slot)
        for n in range(hid.shape[1] // tile):
            cols = pl.ds(n * tile, tile)
            for acc, w in ((g_acc, w_gate), (u_acc, w_up)):
                total = dot(xin[rows, own], w[own, cols])
                for q in (px, py):
                    total += dot(xin[rows, cols_of(q)], w[cols_of(q), cols])
                acc[:, cols] = total

    def gate_up_rest(g):
        rows = pl.ds(2 * g * slot, 2 * slot)
        for n in range(hid.shape[1] // tile):
            cols = pl.ds(n * tile, tile)
            gate = g_acc[:, cols] + dot(xin[rows, far], w_gate[far, cols])
            up = u_acc[:, cols] + dot(xin[rows, far], w_up[far, cols])
            hid[rows, cols] = (silu(gate) * up).astype(bf16)

    def gate_up(g, count=1, tiles=None):
        rows = pl.ds(2 * g * slot, 2 * count * slot)
        for n in tiles or range(hid.shape[1] // tile):
            cols = pl.ds(n * tile, tile)
            gate = dot(xin[rows, :], w_gate[:, cols])
            up = dot(xin[rows, :], w_up[:, cols])
            hid[rows, cols] = (silu(gate) * up).astype(bf16)

    def down(g, count, *slots):
        rows = pl.ds(2 * g * slot, 2 * count * slot)
        for to in slots:
            q = (p, px, py, pd)[to]
            for n in range(width // tile):
                src = pl.ds(pl.multiple_of(q * width + n * tile, tile), tile)
                part[to, rows, pl.ds(n * tile, tile)] = dot(
                    hid[rows, :], w_down[:, src]
                ).astype(bf16)

    def spread(pos):
        ref = xin.at[at(pos), own]
        arrive(ref, z_sem.at[pos])
        send(ref, ref, ag_sem.at[0, pos], to_x)
        send(ref, ref, ag_sem.at[1, pos], to_y)

    def forward(pos):
        if pos % 2 == 0:
            ref = xin.at[at(pos), cols_of(px)]
            arrive(ref, ag_sem.at[0, pos])
            send(ref, ref, ag_sem.at[2, pos], to_y)
        else:
            ref = xin.at[at(pos), cols_of(py)]
            arrive(ref, ag_sem.at[1, pos])
            send(ref, ref, ag_sem.at[2, pos], to_x)

    def gathered_xy(g):
        even, odd = 2 * g, 2 * g + 1
        arrive(xin.at[at(odd), cols_of(px)], ag_sem.at[0, odd])
        arrive(xin.at[at(even), cols_of(py)], ag_sem.at[1, even])

    def gathered_d(g):
        for pos in (2 * g, 2 * g + 1):
            arrive(xin.at[at(pos), far], ag_sem.at[2, pos])

    def first(g):
        even, odd = at(2 * g), at(2 * g + 1)
        send(part.at[3, odd], d_in.at[odd], rsd_sem.at[2 * g + 1], to_x)
        send(part.at[3, even], d_in.at[even], rsd_sem.at[2 * g], to_y)

    def direct(g):
        even, odd = at(2 * g), at(2 * g + 1)
        send(part.at[1, odd], rx.at[odd], rsx_sem.at[2 * g + 1], to_x)
        send(part.at[2, even], ry.at[even], rsy_sem.at[2 * g], to_y)

    def joined(g):
        for pos, src, dst, sem, there in (
            (2 * g, 1, rx, rsx_sem, to_x),
            (2 * g + 1, 2, ry, rsy_sem, to_y),
        ):
            b = at(pos)
            arrive(d_in.at[b], rsd_sem.at[pos])
            pair[b, :] = (part[src, b, :].astype(f32) + d_in[b, :].astype(f32)).astype(bf16)
            send(pair.at[b], dst.at[b], sem.at[pos], there)

    def finish(g):
        for c in range(2):
            pos = 2 * g + c
            b = at(pos)
            arrive(rx.at[b], rsx_sem.at[pos])
            arrive(ry.at[b], rsy_sem.at[pos])
            total = (
                part[0, b, :].astype(f32) + rx[b, :].astype(f32) + ry[b, :].astype(f32)
            ).astype(bf16)
            if pos == 0:
                back[block(e), :] = total
            else:
                fin[b, :] = total
                owner = partner if g == 0 else 2 * chips[g] + c
                send(fin.at[b], back.at[block(e)], ret_sem.at[e], {"ep": owner})

    half = tok_rows // 2

    def dense_branch():
        arrive(dhid.at[pd, pl.ds(0, half)], dh_sem.at[2])
        arrive(dhid.at[pd, pl.ds(half, half)], dh_sem.at[3])
        loads[5].wait()
        loads[8].wait()
        total = dot(dhid[0], w_dout[pl.ds(0, side)])
        for q in range(1, dhid.shape[0]):
            total += dot(dhid[q], w_dout[pl.ds(q * side, side)])
        logit = jnp.sum(
            tok[...].astype(f32) * dgate_ref[...].reshape(1, tok.shape[1]).astype(f32),
            axis=1,
            keepdims=True,
        )
        dense[...] = total / (1.0 + jnp.exp(-logit))

    with scope("in0"):
        arrive(xin.at[at(1)], z_sem.at[1])
        loads[2].wait()
        loads[3].wait()
    n_tiles = hid.shape[1] // tile
    with scope("gu0a"):
        gate_up(0, 1, range(n_tiles // 2))
    pl.when(inner == 1)(far_sends)
    with scope("gu0b"):
        gate_up(0, 1, range(n_tiles // 2, n_tiles))
    with scope("down0"):
        loads[4].wait()
        down(0, 1, 3)
        first(0)
        down(0, 1, 1, 2)
        direct(0)
        down(0, 1, 0)
    with scope("spread1"):
        spread(2)
        spread(3)
    with scope("comb"):
        combine_weights()
    with scope("spread2"):
        spread(4)
        spread(5)
    with scope("join0"):
        joined(0)
    with scope("fwd1"):
        forward(2)
        forward(3)
    with scope("dh_fwd"):
        arrive(dhid.at[px], dh_sem.at[0])
        ref = dhid.at[px, pl.ds(0, half)]
        send(ref, ref, dh_sem.at[2], to_y)
        arrive(dhid.at[py], dh_sem.at[1])
        ref = dhid.at[py, pl.ds(half, half)]
        send(ref, ref, dh_sem.at[3], to_x)
    with scope("in1xy"):
        gathered_xy(1)
    with scope("gu1p"):
        gate_up_part(1)
    with scope("fwd2"):
        forward(4)
        forward(5)
    with scope("in1d"):
        gathered_d(1)
    with scope("gu1r"):
        gate_up_rest(1)
    with scope("down1"):
        down(1, 1, 3)
        first(1)
        down(1, 1, 1, 2)
        direct(1)
        down(1, 1, 0)
    with scope("in3"):
        arrive(xin.at[at(6)], z_sem.at[6])
        arrive(xin.at[at(7)], z_sem.at[7])
    with scope("in2"):
        gathered_xy(2)
        gathered_d(2)
    with scope("gu2"):
        gate_up(2, 2)
    with scope("join1"):
        joined(1)
    with scope("down2"):
        down(2, 2, 3)
        first(2)
        first(3)
        down(2, 2, 1, 2)
        direct(2)
        direct(3)
        down(2, 2, 0)
    with scope("fin1"):
        finish(1)
    with scope("dense"):
        dense_branch()
    with scope("join2"):
        joined(2)
    with scope("join3"):
        joined(3)
    with scope("fin0"):
        finish(0)
    with scope("fin2"):
        finish(2)
    with scope("fin3"):
        finish(3)
    with scope("ret"):
        for k in range(1, n_ep):
            owner = (e + n_ep - k) % n_ep
            arrive(back.at[block(owner)], ret_sem.at[owner])
    with scope("out"):
        out_ref[...] = dense[...] + dot(comb[0], back[...]) + dot(comb[1], back[...])
    with scope("drain"):
        for copy in sends + crossing:
            copy.wait_send()


def fused_per_device(
    tokens,
    gate_proj,
    up_proj,
    down_proj,
    side_input_weight,
    dense_out,
    dense_gate,
    chosen_rows,
    choice_weights,
):
    n_ep, slot = chosen_rows.shape
    n_tp = lax.axis_size("tp")
    tok_rows, d = tokens.shape
    width = d // n_tp
    ff = gate_proj.shape[2]
    side = side_input_weight.shape[1]
    cap = n_ep * slot
    bf16, f32 = jnp.bfloat16, jnp.float32
    n_sends = 2 + 1 + 4 + 8 + 4 + 3 * n_ep + n_ep - 1
    hbm = pl.BlockSpec(memory_space=pltpu.HBM)
    vmem = pl.BlockSpec(memory_space=pltpu.VMEM)
    return pl.pallas_call(
        functools.partial(layer_kernel, slot),
        out_shape=pltpu.VMEM((tok_rows, width), f32),
        in_specs=[hbm] * 9,
        out_specs=vmem,
        scratch_shapes=[
            pltpu.VMEM(dense_gate.shape, bf16),
            pltpu.VMEM(chosen_rows.shape, jnp.int32),
            pltpu.VMEM(choice_weights.shape, f32),
            pltpu.VMEM((tok_rows, d), bf16),
            pltpu.VMEM((d, ff), bf16),
            pltpu.VMEM((d, ff), bf16),
            pltpu.VMEM((ff, d), bf16),
            pltpu.VMEM((d, side), bf16),
            pltpu.VMEM((n_tp * side, width), bf16),
            pltpu.VMEM((cap, d), bf16),
            pltpu.VMEM((cap, d), bf16),
            pltpu.VMEM((2 * slot, ff), f32),
            pltpu.VMEM((2 * slot, ff), f32),
            pltpu.VMEM((cap, ff), bf16),
            pltpu.VMEM((2, tok_rows, cap), bf16),
            pltpu.VMEM((n_tp, tok_rows, side), bf16),
            pltpu.VMEM((tok_rows, width), f32),
            pltpu.VMEM((4, cap, width), bf16),
            pltpu.VMEM((cap, width), bf16),
            pltpu.VMEM((cap, width), bf16),
            pltpu.VMEM((cap, width), bf16),
            pltpu.VMEM((cap, width), bf16),
            pltpu.VMEM((cap, width), bf16),
            pltpu.VMEM((cap, width), bf16),
            pltpu.SemaphoreType.DMA((9,)),
            pltpu.SemaphoreType.DMA((n_sends,)),
            pltpu.SemaphoreType.DMA((4,)),
            pltpu.SemaphoreType.DMA((n_ep,)),
            pltpu.SemaphoreType.DMA((3, n_ep)),
            pltpu.SemaphoreType.DMA((4,)),
            pltpu.SemaphoreType.DMA((n_ep,)),
            pltpu.SemaphoreType.DMA((n_ep,)),
            pltpu.SemaphoreType.DMA((n_ep,)),
            pltpu.SemaphoreType.DMA((n_ep,)),
        ],
        compiler_params=pltpu.CompilerParams(collective_id=0, has_side_effects=True),
    )(
        tokens,
        gate_proj,
        up_proj,
        down_proj,
        side_input_weight,
        dense_out,
        dense_gate,
        chosen_rows,
        choice_weights,
    ).astype(bf16)


def per_device(*args):
    tokens, gate_proj, chosen_rows = args[0], args[1], args[7]
    n_ep, slot = chosen_rows.shape
    n_tp = lax.axis_size("tp")
    width, tile = tokens.shape[1] // n_tp, 2 * LANES
    fits = (
        n_tp == 4
        and n_ep == 8
        and tokens.shape[0] == n_ep * slot
        and slot % 16 == 0
        and width % tile == 0
        and gate_proj.shape[2] % tile == 0
        and args[4].shape[1] % LANES == 0
    )
    return fused_per_device(*args) if fits else plain_per_device(*args)


def solution(mesh):
    placed = (
        P("ep", None),
        P("ep", None, "tp"),
        P("ep", None, "tp"),
        P("ep", "tp", None),
        P(None, "tp"),
        P(None, "tp"),
        P(),
        P(None, "ep"),
        P(None, "ep"),
    )
    return jax.shard_map(
        per_device, mesh=mesh, in_specs=placed, out_specs=P("ep", "tp"), check_vma=False
    )
```

time: 38.8 us -> 34.7 us (0.89)
  Pallas kernels: 37.9 us -> 33.8 us
    pallas_call x1, Pallas kernels: 37.9 us -> 33.8 us  [fused_per_device(): pl.pallas_call(functools.partial(layer_kernel, slot), out_shape=pltpu.VME...]
where the time goes in v1:
time: 34.7 us; the launch traced here: 34.5 us
  Pallas kernels  33.8 us (97%)
  other arithmetic  0.74 us (2%)
    pallas_call x1, Pallas kernels, fused_per_device(): pl.pallas_call(functools.partial(layer_kernel, slot), out_shape=pltpu.VME...  33.8 us
    convert_element_type x1, other arithmetic, fused_per_device(): return pl.pallas_call(functools.partial(layer_kernel, slot), out_shape=pl...  0.74 us

profile of v1, /device:TPU:0, one launch (start us, length us, event | category | flops | bytes accessed | tf_op | source)
XLA Modules:
  0.0 34.5 jit_solution(17305428072283466342)
XLA Ops:
  0.0 33.8 %shard_map.91 = f32[256,512]{1,0:T(8,128)S(1)} custom-call(bf16[256,2048]{1,0:T(8,128)(2,1)} %tok_hbm.1, bf16[1,2048,1024]{2,1,0:T(8,128)(2,1)} %gate_hbm.1, bf16[1,2048,1024]{2,1,0:T(8,128)(2,1)} %up_hbm.1, bf16[1,1024,2048]{2,1,0:T(8,128)(2,1)} %down_hbm.1, bf16[2048,256]{1,0:T(8,128)(2,1)} %side_hbm.1, bf16[1024,512]{1,0:T(8,128)(2,1)} %dout_hbm.1, ...), custom_call_target="tpu_custom_call" | custom-call | tf_op jit(solution)/shard_map/pallas_call | solution.py:502
  33.8 0.7 %convert_element_type.3 = bf16[256,512]{1,0:T(8,128)(2,1)} convert(f32[256,512]{1,0:T(8,128)S(1)} %shard_map.91) | non-fusion elementwise | flops 131072 | bytes 786432 | tf_op jit(solution)/shard_map/convert_element_type | solution.py:554

commit v2 on v1

--- a/solution.py
+++ b/solution.py
@@ -115,7 +115,6 @@
     back,
     load_sem,
     send_sem,
-    far_sem,
     z_sem,
     ag_sem,
     dh_sem,
@@ -136,25 +135,38 @@
     upper = z // 2
     inner = (z + upper) % 2
     chips = [z, 3 - 3 * upper, 2 - upper, z + 1 - 2 * (z % 2)]
+    near, late, mate = 1, 2, 3
+    direct_in, direct_out = (), ()
     width = out_ref.shape[1]
     tok_rows = tok.shape[0]
     side = w_side.shape[1]
-    to_x, to_y = {"tp": px}, {"tp": py}
+    to_x, to_y, to_d = {"tp": px}, {"tp": py}, {"tp": pd}
     f32, bf16 = jnp.float32, jnp.bfloat16
     scope = jax.named_scope
+
+    def block(owner):
+        return pl.ds(pl.multiple_of(owner * slot, slot), slot)
+
+    def at(pos):
+        return pl.ds(pos * slot, slot)
+
+    def cols_of(q):
+        return pl.ds(pl.multiple_of(q * width, width), width)
+
+    own, far = cols_of(p), cols_of(pd)
 
     barrier = pltpu.get_barrier_semaphore()
     for k in range(1, n_ep):
         pl.semaphore_signal(
             barrier, inc=1, device_id={"ep": (e + k) % n_ep}, device_id_type=MESH
         )
-    for there in (to_x, to_y):
+    for there in (to_x, to_y, to_d):
         pl.semaphore_signal(barrier, inc=1, device_id=there, device_id_type=MESH)
 
     loads = []
     for i, (src, dst) in enumerate(
         (
-            (tok_hbm, tok),
+            (tok_hbm.at[:, own], tok.at[:, own]),
             (side_hbm, w_side),
             (gate_hbm.at[0], w_gate),
             (up_hbm.at[0], w_up),
@@ -163,20 +175,12 @@
             (rows_hbm, rows_ref),
             (cw_hbm, cw_ref),
             (dgate_hbm, dgate_ref),
+            *((tok_hbm.at[:, cols_of(q)], tok.at[:, cols_of(q)]) for q in (px, py, pd)),
         )
     ):
         loads.append(pltpu.make_async_copy(src, dst, load_sem.at[i]))
-    for i in (6, 0, 1, 7, 8, 2, 3, 4, 5):
+    for i in (6, 0, 9, 10, 11, 1, 7, 8, 2, 3, 4, 5):
         loads[i].start()
-
-    def block(owner):
-        return pl.ds(pl.multiple_of(owner * slot, slot), slot)
-
-    def at(pos):
-        return pl.ds(pos * slot, slot)
-
-    def cols_of(q):
-        return pl.ds(pl.multiple_of(q * width, width), width)
 
     sends = []
 
@@ -212,42 +216,28 @@
         chosen = hits.astype(bf16)
         loads[0].wait()
     with scope("pick"):
-        for q in range(tok.shape[1] // width):
-            cols = pl.ds(q * width, width)
-            pick[:, cols] = dot(chosen, tok[:, cols]).astype(bf16)
+        pick[:, own] = dot(chosen, tok[:, own]).astype(bf16)
     with scope("barrier"):
-        pl.semaphore_wait(barrier, n_ep + 1)
-
-    own, far = cols_of(p), cols_of(pd)
+        pl.semaphore_wait(barrier, n_ep + 2)
 
     def slot_of(pos):
         return pl.ds(pl.multiple_of(pos * slot, slot), slot)
 
-    crossing = []
-    for i, (g, c) in enumerate(((1, 0), (1, 1), (2, 0), (2, 1))):
-        peer = 2 * chips[g] + c
-        pos = 2 * (1 + inner) + core
-        crossing.append(
-            pltpu.make_async_remote_copy(
-                src_ref=pick.at[block(peer), own],
-                dst_ref=xin.at[slot_of(pos), own],
-                send_sem=far_sem.at[i],
-                recv_sem=z_sem.at[pos],
-                device_id={"ep": peer},
-                device_id_type=MESH,
-            )
-        )
-
-    def far_sends():
-        for copy in crossing:
-            copy.start()
-
-    pl.when(inner == 0)(far_sends)
+    for g in (near, late):
+        for c in range(2):
+            peer = 2 * chips[g] + c
+            pos = 2 * (near + inner) + core
+            dst = xin.at[slot_of(pos), own]
+            send(pick.at[block(peer), own], dst, z_sem.at[pos], {"ep": peer})
+    with scope("pick2"):
+        for i, q in enumerate((px, py, pd)):
+            loads[9 + i].wait()
+            pick[:, cols_of(q)] = dot(chosen, tok[:, cols_of(q)]).astype(bf16)
+    send(pick.at[block(partner)], xin.at[at(1)], z_sem.at[1], {"ep": partner})
     for c in range(2):
-        peer = 2 * chips[3] + c
-        pos = 6 + core
+        peer = 2 * chips[mate] + c
+        pos = 2 * mate + core
         send(pick.at[block(peer)], xin.at[slot_of(pos)], z_sem.at[pos], {"ep": peer})
-    send(pick.at[block(partner)], xin.at[at(1)], z_sem.at[1], {"ep": partner})
     with scope("dhid"):
         loads[1].wait()
         dhid[p] = silu(dot(tok[...], w_side[...])).astype(bf16)
@@ -266,22 +256,22 @@
 
     tile = 2 * LANES
 
-    def gate_up_part(g):
-        rows = pl.ds(2 * g * slot, 2 * slot)
+    def gate_up_part(g, count):
+        rows = pl.ds(2 * g * slot, 2 * count * slot)
         for n in range(hid.shape[1] // tile):
             cols = pl.ds(n * tile, tile)
             for acc, w in ((g_acc, w_gate), (u_acc, w_up)):
                 total = dot(xin[rows, own], w[own, cols])
                 for q in (px, py):
                     total += dot(xin[rows, cols_of(q)], w[cols_of(q), cols])
-                acc[:, cols] = total
-
-    def gate_up_rest(g):
-        rows = pl.ds(2 * g * slot, 2 * slot)
+                acc[rows, cols] = total
+
+    def gate_up_rest(g, count):
+        rows = pl.ds(2 * g * slot, 2 * count * slot)
         for n in range(hid.shape[1] // tile):
             cols = pl.ds(n * tile, tile)
-            gate = g_acc[:, cols] + dot(xin[rows, far], w_gate[far, cols])
-            up = u_acc[:, cols] + dot(xin[rows, far], w_up[far, cols])
+            gate = g_acc[rows, cols] + dot(xin[rows, far], w_gate[far, cols])
+            up = u_acc[rows, cols] + dot(xin[rows, far], w_up[far, cols])
             hid[rows, cols] = (silu(gate) * up).astype(bf16)
 
     def gate_up(g, count=1, tiles=None):
@@ -302,42 +292,55 @@
                     hid[rows, :], w_down[:, src]
                 ).astype(bf16)
 
-    def spread(pos):
-        ref = xin.at[at(pos), own]
-        arrive(ref, z_sem.at[pos])
-        send(ref, ref, ag_sem.at[0, pos], to_x)
-        send(ref, ref, ag_sem.at[1, pos], to_y)
-
-    def forward(pos):
-        if pos % 2 == 0:
-            ref = xin.at[at(pos), cols_of(px)]
-            arrive(ref, ag_sem.at[0, pos])
-            send(ref, ref, ag_sem.at[2, pos], to_y)
-        else:
-            ref = xin.at[at(pos), cols_of(py)]
-            arrive(ref, ag_sem.at[1, pos])
-            send(ref, ref, ag_sem.at[2, pos], to_x)
+    def spread(g):
+        even, odd = 2 * g, 2 * g + 1
+        for pos in (even, odd):
+            arrive(xin.at[at(pos), own], z_sem.at[pos])
+        order = ((even, 0), (odd, 1), (odd, 0), (even, 1))
+        if g in direct_in:
+            order = ((even, 2), (odd, 2)) + order
+        for pos, axis in order:
+            ref = xin.at[at(pos), own]
+            send(ref, ref, ag_sem.at[axis, pos], (to_x, to_y, to_d)[axis])
+
+    def forward(g):
+        if g in direct_in:
+            return
+        even, odd = 2 * g, 2 * g + 1
+        for pos, axis, q, there in ((even, 0, px, to_y), (odd, 1, py, to_x)):
+            ref = xin.at[at(pos), cols_of(q)]
+            arrive(ref, ag_sem.at[axis, pos])
+            send(ref, ref, ag_sem.at[2, pos], there)
 
     def gathered_xy(g):
         even, odd = 2 * g, 2 * g + 1
-        arrive(xin.at[at(odd), cols_of(px)], ag_sem.at[0, odd])
-        arrive(xin.at[at(even), cols_of(py)], ag_sem.at[1, even])
+        for pos in (even, odd):
+            if g in direct_in or pos == odd:
+                arrive(xin.at[at(pos), cols_of(px)], ag_sem.at[0, pos])
+            if g in direct_in or pos == even:
+                arrive(xin.at[at(pos), cols_of(py)], ag_sem.at[1, pos])
 
     def gathered_d(g):
         for pos in (2 * g, 2 * g + 1):
             arrive(xin.at[at(pos), far], ag_sem.at[2, pos])
 
     def first(g):
-        even, odd = at(2 * g), at(2 * g + 1)
-        send(part.at[3, odd], d_in.at[odd], rsd_sem.at[2 * g + 1], to_x)
-        send(part.at[3, even], d_in.at[even], rsd_sem.at[2 * g], to_y)
+        for pos, there in ((2 * g + 1, to_x), (2 * g, to_y)):
+            there = to_d if g in direct_out else there
+            send(part.at[3, at(pos)], d_in.at[at(pos)], rsd_sem.at[pos], there)
 
     def direct(g):
-        even, odd = at(2 * g), at(2 * g + 1)
-        send(part.at[1, odd], rx.at[odd], rsx_sem.at[2 * g + 1], to_x)
-        send(part.at[2, even], ry.at[even], rsy_sem.at[2 * g], to_y)
+        even, odd = 2 * g, 2 * g + 1
+        for pos in (odd, even):
+            b = at(pos)
+            if g in direct_out or pos == odd:
+                send(part.at[1, b], rx.at[b], rsx_sem.at[pos], to_x)
+            if g in direct_out or pos == even:
+                send(part.at[2, b], ry.at[b], rsy_sem.at[pos], to_y)
 
     def joined(g):
+        if g in direct_out:
+            return
         for pos, src, dst, sem, there in (
             (2 * g, 1, rx, rsx_sem, to_x),
             (2 * g + 1, 2, ry, rsy_sem, to_y),
@@ -353,13 +356,14 @@
             b = at(pos)
             arrive(rx.at[b], rsx_sem.at[pos])
             arrive(ry.at[b], rsy_sem.at[pos])
-            total = (
-                part[0, b, :].astype(f32) + rx[b, :].astype(f32) + ry[b, :].astype(f32)
-            ).astype(bf16)
+            total = part[0, b, :].astype(f32) + rx[b, :].astype(f32) + ry[b, :].astype(f32)
+            if g in direct_out:
+                arrive(d_in.at[b], rsd_sem.at[pos])
+                total += d_in[b, :].astype(f32)
             if pos == 0:
-                back[block(e), :] = total
+                back[block(e), :] = total.astype(bf16)
             else:
-                fin[b, :] = total
+                fin[b, :] = total.astype(bf16)
                 owner = partner if g == 0 else 2 * chips[g] + c
                 send(fin.at[b], back.at[block(e)], ret_sem.at[e], {"ep": owner})
 
@@ -387,7 +391,6 @@
     n_tiles = hid.shape[1] // tile
     with scope("gu0a"):
         gate_up(0, 1, range(n_tiles // 2))
-    pl.when(inner == 1)(far_sends)
     with scope("gu0b"):
         gate_up(0, 1, range(n_tiles // 2, n_tiles))
     with scope("down0"):
@@ -397,19 +400,18 @@
         down(0, 1, 1, 2)
         direct(0)
         down(0, 1, 0)
-    with scope("spread1"):
-        spread(2)
-        spread(3)
+    with scope("spreadA"):
+        spread(near)
     with scope("comb"):
         combine_weights()
-    with scope("spread2"):
-        spread(4)
-        spread(5)
+    with scope("spreadB"):
+        spread(late)
+    with scope("fwdA"):
+        forward(near)
     with scope("join0"):
         joined(0)
-    with scope("fwd1"):
-        forward(2)
-        forward(3)
+    with scope("fwdB"):
+        forward(late)
     with scope("dh_fwd"):
         arrive(dhid.at[px], dh_sem.at[0])
         ref = dhid.at[px, pl.ds(0, half)]
@@ -417,63 +419,71 @@
         arrive(dhid.at[py], dh_sem.at[1])
         ref = dhid.at[py, pl.ds(half, half)]
         send(ref, ref, dh_sem.at[3], to_x)
-    with scope("in1xy"):
-        gathered_xy(1)
-    with scope("gu1p"):
-        gate_up_part(1)
-    with scope("fwd2"):
-        forward(4)
-        forward(5)
-    with scope("in1d"):
-        gathered_d(1)
-    with scope("gu1r"):
-        gate_up_rest(1)
-    with scope("down1"):
-        down(1, 1, 3)
-        first(1)
-        down(1, 1, 1, 2)
-        direct(1)
-        down(1, 1, 0)
-    with scope("in3"):
-        arrive(xin.at[at(6)], z_sem.at[6])
-        arrive(xin.at[at(7)], z_sem.at[7])
-    with scope("in2"):
-        gathered_xy(2)
-        gathered_d(2)
-    with scope("gu2"):
-        gate_up(2, 2)
-    with scope("join1"):
-        joined(1)
-    with scope("down2"):
-        down(2, 2, 3)
-        first(2)
-        first(3)
-        down(2, 2, 1, 2)
-        direct(2)
-        direct(3)
-        down(2, 2, 0)
-    with scope("fin1"):
-        finish(1)
+    with scope("inAxy"):
+        gathered_xy(near)
+    with scope("guAp"):
+        gate_up_part(near, 1)
+    with scope("inP"):
+        for c in range(2):
+            arrive(xin.at[at(2 * mate + c)], z_sem.at[2 * mate + c])
+    with scope("inBxy"):
+        gathered_xy(late)
+    with scope("guBp"):
+        gate_up_part(late, 2)
+    with scope("inAd"):
+        gathered_d(near)
+    with scope("guAr"):
+        gate_up_rest(near, 1)
+    with scope("downA"):
+        down(near, 1, 3)
+        first(near)
+        down(near, 1, 1, 2)
+        direct(near)
+    with scope("inBd"):
+        gathered_d(late)
+    with scope("guBr"):
+        gate_up_rest(late, 2)
+    with scope("downB"):
+        down(late, 2, 3)
+        first(mate)
+        first(late)
+        down(late, 2, 1, 2)
+        down(near, 1, 0)
+    with scope("joinA"):
+        joined(near)
+    direct(mate)
+    with scope("downB0"):
+        down(late, 2, 0)
+    with scope("joinP"):
+        joined(mate)
+    direct(late)
+    with scope("joinB"):
+        joined(late)
+    with scope("finA"):
+        finish(near)
+    with scope("fin0"):
+        finish(0)
+    with scope("finP"):
+        finish(mate)
+    with scope("finB"):
+        finish(late)
     with scope("dense"):
         dense_branch()
-    with scope("join2"):
-        joined(2)
-    with scope("join3"):
-        joined(3)
-    with scope("fin0"):
-        finish(0)
-    with scope("fin2"):
-        finish(2)
-    with scope("fin3"):
-        finish(3)
-    with scope("ret"):
-        for k in range(1, n_ep):
-            owner = (e + n_ep - k) % n_ep
-            arrive(back.at[block(owner)], ret_sem.at[owner])
+    def returned(owner):
+        arrive(back.at[block(owner)], ret_sem.at[owner])
+
+    with scope("ret0"):
+        returned(partner)
+    for g in (near, mate, late):
+        with scope(f"ret{'xABP'[g]}"):
+            for c in range(2):
+                returned(2 * chips[g] + c)
     with scope("out"):
-        out_ref[...] = dense[...] + dot(comb[0], back[...]) + dot(comb[1], back[...])
+        out_ref[...] = (
+            dense[...] + dot(comb[0], back[...]) + dot(comb[1], back[...])
+        ).astype(bf16)
     with scope("drain"):
-        for copy in sends + crossing:
+        for copy in sends:
             copy.wait_send()
 
 
@@ -496,12 +506,12 @@
     side = side_input_weight.shape[1]
     cap = n_ep * slot
     bf16, f32 = jnp.bfloat16, jnp.float32
-    n_sends = 2 + 1 + 4 + 8 + 4 + 3 * n_ep + n_ep - 1
+    n_sends = (n_ep - 1) + 4 + 3 * (n_ep - 4) + 3 * n_ep + (n_ep - 1)
     hbm = pl.BlockSpec(memory_space=pltpu.HBM)
     vmem = pl.BlockSpec(memory_space=pltpu.VMEM)
     return pl.pallas_call(
         functools.partial(layer_kernel, slot),
-        out_shape=pltpu.VMEM((tok_rows, width), f32),
+        out_shape=pltpu.VMEM((tok_rows, width), bf16),
         in_specs=[hbm] * 9,
         out_specs=vmem,
         scratch_shapes=[
@@ -516,8 +526,8 @@
             pltpu.VMEM((n_tp * side, width), bf16),
             pltpu.VMEM((cap, d), bf16),
             pltpu.VMEM((cap, d), bf16),
-            pltpu.VMEM((2 * slot, ff), f32),
-            pltpu.VMEM((2 * slot, ff), f32),
+            pltpu.VMEM((cap, ff), f32),
+            pltpu.VMEM((cap, ff), f32),
             pltpu.VMEM((cap, ff), bf16),
             pltpu.VMEM((2, tok_rows, cap), bf16),
             pltpu.VMEM((n_tp, tok_rows, side), bf16),
@@ -529,9 +539,8 @@
             pltpu.VMEM((cap, width), bf16),
             pltpu.VMEM((cap, width), bf16),
             pltpu.VMEM((cap, width), bf16),
-            pltpu.SemaphoreType.DMA((9,)),
+            pltpu.SemaphoreType.DMA((12,)),
             pltpu.SemaphoreType.DMA((n_sends,)),
-            pltpu.SemaphoreType.DMA((4,)),
             pltpu.SemaphoreType.DMA((n_ep,)),
             pltpu.SemaphoreType.DMA((3, n_ep)),
             pltpu.SemaphoreType.DMA((4,)),
@@ -551,7 +560,7 @@
         dense_gate,
         chosen_rows,
         choice_weights,
-    ).astype(bf16)
+    )
 
 
 def per_device(*args):

time: 34.7 us -> 32.2 us (0.928)
  Pallas kernels: 33.8 us -> 31.3 us
  other arithmetic: 0.74 us -> 0 us
  local copies, waits for them, and re-layouts: 0 us -> 0.71 us
    pallas_call x1, Pallas kernels: 33.8 us -> 31.3 us  [fused_per_device(): pl.pallas_call(functools.partial(layer_kernel, slot), out_shape=pltpu.VME...]
    convert_element_type x1 -> x0, other arithmetic: 0.74 us -> none  [fused_per_device(): return pl.pallas_call(functools.partial(layer_kernel, slot), out_shape=pl...]
    unnamed x0 -> x1, local copies, waits for them, and re-layouts: none -> 0.71 us
where the time goes in v2:
time: 32.2 us; the launch traced here: 32 us
  Pallas kernels  31.3 us (97%)
  local copies, waits for them, and re-layouts  0.71 us (2%)
    pallas_call x1, Pallas kernels, fused_per_device(): pl.pallas_call(functools.partial(layer_kernel, slot), out_shape=pltpu.VME...  31.3 us
    unnamed x1, local copies, waits for them, and re-layouts  0.71 us

profile of v2, /device:TPU:0, one launch (start us, length us, event | category | flops | bytes accessed | tf_op | source)
XLA Modules:
  0.0 32.0 jit_solution(5296943768833329962)
XLA Ops:
  0.0 31.3 %shard_map.91 = bf16[256,512]{1,0:T(8,128)(2,1)S(1)} custom-call(bf16[256,2048]{1,0:T(8,128)(2,1)} %tok_hbm.1, bf16[1,2048,1024]{2,1,0:T(8,128)(2,1)} %gate_hbm.1, bf16[1,2048,1024]{2,1,0:T(8,128)(2,1)} %up_hbm.1, bf16[1,1024,2048]{2,1,0:T(8,128)(2,1)} %down_hbm.1, bf16[2048,256]{1,0:T(8,128)(2,1)} %side_hbm.1, bf16[1024,512]{1,0:T(8,128)(2,1)} %dout_hbm.1, ...), custom_call_target="tpu_custom_call" | custom-call | tf_op jit(solution)/shard_map/pallas_call | solution.py:512
  31.3 0.7 %copy.11 = bf16[256,512]{1,0:T(8,128)(2,1)} copy(bf16[256,512]{1,0:T(8,128)(2,1)S(1)} %shard_map.91) | data formatting | bytes 524288

commit v3 on v2

--- a/solution.py
+++ b/solution.py
@@ -1,4 +1,5 @@
 import functools
+import math
 
 import jax
 import jax.numpy as jnp
@@ -118,9 +119,8 @@
     z_sem,
     ag_sem,
     dh_sem,
-    rsd_sem,
-    rsx_sem,
-    rsy_sem,
+    d_sem,
+    sum_sem,
     ret_sem,
 ):
     n_ep = rows_ref.shape[0]
@@ -136,11 +136,10 @@
     inner = (z + upper) % 2
     chips = [z, 3 - 3 * upper, 2 - upper, z + 1 - 2 * (z % 2)]
     near, late, mate = 1, 2, 3
-    direct_in, direct_out = (), ()
     width = out_ref.shape[1]
     tok_rows = tok.shape[0]
     side = w_side.shape[1]
-    to_x, to_y, to_d = {"tp": px}, {"tp": py}, {"tp": pd}
+    to_x, to_y = {"tp": px}, {"tp": py}
     f32, bf16 = jnp.float32, jnp.bfloat16
     scope = jax.named_scope
 
@@ -160,7 +159,7 @@
         pl.semaphore_signal(
             barrier, inc=1, device_id={"ep": (e + k) % n_ep}, device_id_type=MESH
         )
-    for there in (to_x, to_y, to_d):
+    for there in (to_x, to_y):
         pl.semaphore_signal(barrier, inc=1, device_id=there, device_id_type=MESH)
 
     loads = []
@@ -178,7 +177,7 @@
             *((tok_hbm.at[:, cols_of(q)], tok.at[:, cols_of(q)]) for q in (px, py, pd)),
         )
     ):
-        loads.append(pltpu.make_async_copy(src, dst, load_sem.at[i]))
+        loads.append(pltpu.make_async_copy(src, dst, load_sem.at[min(i, 9)]))
     for i in (6, 0, 9, 10, 11, 1, 7, 8, 2, 3, 4, 5):
         loads[i].start()
 
@@ -188,13 +187,13 @@
         copy = pltpu.make_async_remote_copy(
             src_ref=src,
             dst_ref=dst,
-            send_sem=send_sem.at[len(sends)],
+            send_sem=send_sem.at[0],
             recv_sem=sem,
             device_id=there,
             device_id_type=MESH,
         )
         copy.start()
-        sends.append(copy)
+        sends.append(math.prod(src.shape))
 
     def arrive(dst, sem):
         pltpu.make_async_remote_copy(
@@ -218,7 +217,7 @@
     with scope("pick"):
         pick[:, own] = dot(chosen, tok[:, own]).astype(bf16)
     with scope("barrier"):
-        pl.semaphore_wait(barrier, n_ep + 2)
+        pl.semaphore_wait(barrier, n_ep + 1)
 
     def slot_of(pos):
         return pl.ds(pl.multiple_of(pos * slot, slot), slot)
@@ -228,21 +227,22 @@
             peer = 2 * chips[g] + c
             pos = 2 * (near + inner) + core
             dst = xin.at[slot_of(pos), own]
-            send(pick.at[block(peer), own], dst, z_sem.at[pos], {"ep": peer})
+            send(pick.at[block(peer), own], dst, z_sem.at[near + inner], {"ep": peer})
     with scope("pick2"):
-        for i, q in enumerate((px, py, pd)):
-            loads[9 + i].wait()
+        rest = tok.at[:, pl.ds(0, tok.shape[1] - width)]
+        pltpu.make_async_copy(rest, rest, load_sem.at[9]).wait()
+        for q in (px, py, pd):
             pick[:, cols_of(q)] = dot(chosen, tok[:, cols_of(q)]).astype(bf16)
-    send(pick.at[block(partner)], xin.at[at(1)], z_sem.at[1], {"ep": partner})
+    send(pick.at[block(partner)], xin.at[at(1)], z_sem.at[0], {"ep": partner})
     for c in range(2):
         peer = 2 * chips[mate] + c
         pos = 2 * mate + core
-        send(pick.at[block(peer)], xin.at[slot_of(pos)], z_sem.at[pos], {"ep": peer})
+        send(pick.at[block(peer)], xin.at[slot_of(pos)], z_sem.at[mate], {"ep": peer})
     with scope("dhid"):
         loads[1].wait()
         dhid[p] = silu(dot(tok[...], w_side[...])).astype(bf16)
     send(dhid.at[p], dhid.at[p], dh_sem.at[0], to_x)
-    send(dhid.at[p], dhid.at[p], dh_sem.at[1], to_y)
+    send(dhid.at[p], dhid.at[p], dh_sem.at[0], to_y)
     xin[at(0), :] = pick[block(e), :]
 
     def combine_weights():
@@ -292,86 +292,64 @@
                     hid[rows, :], w_down[:, src]
                 ).astype(bf16)
 
+    def both(g):
+        return pl.ds(2 * g * slot, 2 * slot)
+
     def spread(g):
         even, odd = 2 * g, 2 * g + 1
-        for pos in (even, odd):
-            arrive(xin.at[at(pos), own], z_sem.at[pos])
-        order = ((even, 0), (odd, 1), (odd, 0), (even, 1))
-        if g in direct_in:
-            order = ((even, 2), (odd, 2)) + order
-        for pos, axis in order:
+        arrive(xin.at[both(g), own], z_sem.at[g])
+        for pos, axis in ((even, 0), (odd, 1), (odd, 0), (even, 1)):
             ref = xin.at[at(pos), own]
-            send(ref, ref, ag_sem.at[axis, pos], (to_x, to_y, to_d)[axis])
+            kind = (pos + axis) % 2
+            send(ref, ref, ag_sem.at[kind, g - near], (to_x, to_y)[axis])
 
     def forward(g):
-        if g in direct_in:
-            return
-        even, odd = 2 * g, 2 * g + 1
-        for pos, axis, q, there in ((even, 0, px, to_y), (odd, 1, py, to_x)):
+        arrive(xin.at[both(g), own], ag_sem.at[0, g - near])
+        for pos, q, there in ((2 * g, px, to_y), (2 * g + 1, py, to_x)):
             ref = xin.at[at(pos), cols_of(q)]
-            arrive(ref, ag_sem.at[axis, pos])
-            send(ref, ref, ag_sem.at[2, pos], there)
+            send(ref, ref, ag_sem.at[2, g - near], there)
 
     def gathered_xy(g):
-        even, odd = 2 * g, 2 * g + 1
-        for pos in (even, odd):
-            if g in direct_in or pos == odd:
-                arrive(xin.at[at(pos), cols_of(px)], ag_sem.at[0, pos])
-            if g in direct_in or pos == even:
-                arrive(xin.at[at(pos), cols_of(py)], ag_sem.at[1, pos])
+        arrive(xin.at[both(g), own], ag_sem.at[1, g - near])
 
     def gathered_d(g):
-        for pos in (2 * g, 2 * g + 1):
-            arrive(xin.at[at(pos), far], ag_sem.at[2, pos])
+        arrive(xin.at[both(g), far], ag_sem.at[2, g - near])
 
     def first(g):
         for pos, there in ((2 * g + 1, to_x), (2 * g, to_y)):
-            there = to_d if g in direct_out else there
-            send(part.at[3, at(pos)], d_in.at[at(pos)], rsd_sem.at[pos], there)
+            send(part.at[3, at(pos)], d_in.at[at(pos)], d_sem.at[g], there)
 
     def direct(g):
-        even, odd = 2 * g, 2 * g + 1
-        for pos in (odd, even):
+        even, odd = at(2 * g), at(2 * g + 1)
+        send(part.at[1, odd], rx.at[odd], sum_sem.at[g], to_x)
+        send(part.at[2, even], ry.at[even], sum_sem.at[g], to_y)
+
+    def joined(g):
+        arrive(d_in.at[both(g)], d_sem.at[g])
+        for pos, src, dst, there in ((2 * g, 1, rx, to_x), (2 * g + 1, 2, ry, to_y)):
             b = at(pos)
-            if g in direct_out or pos == odd:
-                send(part.at[1, b], rx.at[b], rsx_sem.at[pos], to_x)
-            if g in direct_out or pos == even:
-                send(part.at[2, b], ry.at[b], rsy_sem.at[pos], to_y)
-
-    def joined(g):
-        if g in direct_out:
-            return
-        for pos, src, dst, sem, there in (
-            (2 * g, 1, rx, rsx_sem, to_x),
-            (2 * g + 1, 2, ry, rsy_sem, to_y),
-        ):
-            b = at(pos)
-            arrive(d_in.at[b], rsd_sem.at[pos])
             pair[b, :] = (part[src, b, :].astype(f32) + d_in[b, :].astype(f32)).astype(bf16)
-            send(pair.at[b], dst.at[b], sem.at[pos], there)
+            send(pair.at[b], dst.at[b], sum_sem.at[g], there)
 
     def finish(g):
+        arrive(d_in.at[pl.ds(0, 4 * slot)], sum_sem.at[g])
         for c in range(2):
             pos = 2 * g + c
             b = at(pos)
-            arrive(rx.at[b], rsx_sem.at[pos])
-            arrive(ry.at[b], rsy_sem.at[pos])
-            total = part[0, b, :].astype(f32) + rx[b, :].astype(f32) + ry[b, :].astype(f32)
-            if g in direct_out:
-                arrive(d_in.at[b], rsd_sem.at[pos])
-                total += d_in[b, :].astype(f32)
+            total = (
+                part[0, b, :].astype(f32) + rx[b, :].astype(f32) + ry[b, :].astype(f32)
+            ).astype(bf16)
             if pos == 0:
-                back[block(e), :] = total.astype(bf16)
+                back[block(e), :] = total
             else:
-                fin[b, :] = total.astype(bf16)
+                fin[b, :] = total
                 owner = partner if g == 0 else 2 * chips[g] + c
-                send(fin.at[b], back.at[block(e)], ret_sem.at[e], {"ep": owner})
+                send(fin.at[b], back.at[block(e)], ret_sem.at[0], {"ep": owner})
 
     half = tok_rows // 2
 
     def dense_branch():
-        arrive(dhid.at[pd, pl.ds(0, half)], dh_sem.at[2])
-        arrive(dhid.at[pd, pl.ds(half, half)], dh_sem.at[3])
+        arrive(dhid.at[pd], dh_sem.at[1])
         loads[5].wait()
         loads[8].wait()
         total = dot(dhid[0], w_dout[pl.ds(0, side)])
@@ -385,7 +363,7 @@
         dense[...] = total / (1.0 + jnp.exp(-logit))
 
     with scope("in0"):
-        arrive(xin.at[at(1)], z_sem.at[1])
+        arrive(xin.at[at(1)], z_sem.at[0])
         loads[2].wait()
         loads[3].wait()
     n_tiles = hid.shape[1] // tile
@@ -413,19 +391,17 @@
     with scope("fwdB"):
         forward(late)
     with scope("dh_fwd"):
-        arrive(dhid.at[px], dh_sem.at[0])
+        arrive(dhid.at[pl.ds(0, 2)], dh_sem.at[0])
         ref = dhid.at[px, pl.ds(0, half)]
-        send(ref, ref, dh_sem.at[2], to_y)
-        arrive(dhid.at[py], dh_sem.at[1])
+        send(ref, ref, dh_sem.at[1], to_y)
         ref = dhid.at[py, pl.ds(half, half)]
-        send(ref, ref, dh_sem.at[3], to_x)
+        send(ref, ref, dh_sem.at[1], to_x)
     with scope("inAxy"):
         gathered_xy(near)
     with scope("guAp"):
         gate_up_part(near, 1)
     with scope("inP"):
-        for c in range(2):
-            arrive(xin.at[at(2 * mate + c)], z_sem.at[2 * mate + c])
+        arrive(xin.at[both(mate)], z_sem.at[mate])
     with scope("inBxy"):
         gathered_xy(late)
     with scope("guBp"):
@@ -469,22 +445,15 @@
         finish(late)
     with scope("dense"):
         dense_branch()
-    def returned(owner):
-        arrive(back.at[block(owner)], ret_sem.at[owner])
-
-    with scope("ret0"):
-        returned(partner)
-    for g in (near, mate, late):
-        with scope(f"ret{'xABP'[g]}"):
-            for c in range(2):
-                returned(2 * chips[g] + c)
+    with scope("ret"):
+        arrive(back.at[pl.ds(0, (n_ep - 1) * slot)], ret_sem.at[0])
     with scope("out"):
         out_ref[...] = (
             dense[...] + dot(comb[0], back[...]) + dot(comb[1], back[...])
         ).astype(bf16)
     with scope("drain"):
-        for copy in sends:
-            copy.wait_send()
+        sent = w_gate.at[pl.ds(0, sum(sends) // w_gate.shape[1])]
+        pltpu.make_async_copy(sent, sent, send_sem.at[0]).wait()
 
 
 def fused_per_device(
@@ -506,7 +475,6 @@
     side = side_input_weight.shape[1]
     cap = n_ep * slot
     bf16, f32 = jnp.bfloat16, jnp.float32
-    n_sends = (n_ep - 1) + 4 + 3 * (n_ep - 4) + 3 * n_ep + (n_ep - 1)
     hbm = pl.BlockSpec(memory_space=pltpu.HBM)
     vmem = pl.BlockSpec(memory_space=pltpu.VMEM)
     return pl.pallas_call(
@@ -539,15 +507,14 @@
             pltpu.VMEM((cap, width), bf16),
             pltpu.VMEM((cap, width), bf16),
             pltpu.VMEM((cap, width), bf16),
-            pltpu.SemaphoreType.DMA((12,)),
-            pltpu.SemaphoreType.DMA((n_sends,)),
-            pltpu.SemaphoreType.DMA((n_ep,)),
-            pltpu.SemaphoreType.DMA((3, n_ep)),
+            pltpu.SemaphoreType.DMA((10,)),
+            pltpu.SemaphoreType.DMA((1,)),
             pltpu.SemaphoreType.DMA((4,)),
-            pltpu.SemaphoreType.DMA((n_ep,)),
-            pltpu.SemaphoreType.DMA((n_ep,)),
-            pltpu.SemaphoreType.DMA((n_ep,)),
-            pltpu.SemaphoreType.DMA((n_ep,)),
+            pltpu.SemaphoreType.DMA((3, 2)),
+            pltpu.SemaphoreType.DMA((2,)),
+            pltpu.SemaphoreType.DMA((4,)),
+            pltpu.SemaphoreType.DMA((4,)),
+            pltpu.SemaphoreType.DMA((1,)),
         ],
         compiler_params=pltpu.CompilerParams(collective_id=0, has_side_effects=True),
     )(
@@ -574,8 +541,9 @@
         and tokens.shape[0] == n_ep * slot
         and slot % 16 == 0
         and width % tile == 0
-        and gate_proj.shape[2] % tile == 0
+        and gate_proj.shape[2] == 2 * width
         and args[4].shape[1] % LANES == 0
+        and 2 * args[4].shape[1] == width
     )
     return fused_per_device(*args) if fits else plain_per_device(*args)
 

time: 32.2 us -> 31.2 us (0.969)
  Pallas kernels: 31.3 us -> 30.3 us
    pallas_call x1, Pallas kernels: 31.3 us -> 30.3 us  [fused_per_device(): pl.pallas_call(functools.partial(layer_kernel, slot), out_shape=pltpu.VME...]
where the time goes in v3:
time: 31.2 us; the launch traced here: 31 us
  Pallas kernels  30.3 us (97%)
  local copies, waits for them, and re-layouts  0.71 us (2%)
    pallas_call x1, Pallas kernels, fused_per_device(): pl.pallas_call(functools.partial(layer_kernel, slot), out_shape=pltpu.VME...  30.3 us
    unnamed x1, local copies, waits for them, and re-layouts  0.71 us

profile of v3, /device:TPU:0, one launch (start us, length us, event | category | flops | bytes accessed | tf_op | source)
XLA Modules:
  0.0 31.0 jit_solution(15261433791006424855)
XLA Ops:
  0.0 30.3 %shard_map.91 = bf16[256,512]{1,0:T(8,128)(2,1)S(1)} custom-call(bf16[256,2048]{1,0:T(8,128)(2,1)} %tok_hbm.1, bf16[1,2048,1024]{2,1,0:T(8,128)(2,1)} %gate_hbm.1, bf16[1,2048,1024]{2,1,0:T(8,128)(2,1)} %up_hbm.1, bf16[1,1024,2048]{2,1,0:T(8,128)(2,1)} %down_hbm.1, bf16[2048,256]{1,0:T(8,128)(2,1)} %side_hbm.1, bf16[1024,512]{1,0:T(8,128)(2,1)} %dout_hbm.1, ...), custom_call_target="tpu_custom_call" | custom-call | tf_op jit(solution)/shard_map/pallas_call | solution.py:480
  30.3 0.7 %copy.11 = bf16[256,512]{1,0:T(8,128)(2,1)} copy(bf16[256,512]{1,0:T(8,128)(2,1)S(1)} %shard_map.91) | data formatting | bytes 524288

commit v4 on v3

--- a/solution.py
+++ b/solution.py
@@ -424,15 +424,15 @@
         first(mate)
         first(late)
         down(late, 2, 1, 2)
-        down(near, 1, 0)
     with scope("joinA"):
         joined(near)
     direct(mate)
     with scope("downB0"):
+        down(near, 1, 0)
         down(late, 2, 0)
+    direct(late)
     with scope("joinP"):
         joined(mate)
-    direct(late)
     with scope("joinB"):
         joined(late)
     with scope("finA"):

time: 31.2 us -> 31.4 us (level)
  no operation moved by 1% of the time
where the time goes in v4:
time: 31.4 us; the launch traced here: 31.2 us
  Pallas kernels  30.5 us (97%)
  local copies, waits for them, and re-layouts  0.71 us (2%)
    pallas_call x1, Pallas kernels, fused_per_device(): pl.pallas_call(functools.partial(layer_kernel, slot), out_shape=pltpu.VME...  30.5 us
    unnamed x1, local copies, waits for them, and re-layouts  0.71 us

profile of v4, /device:TPU:0, one launch (start us, length us, event | category | flops | bytes accessed | tf_op | source)
XLA Modules:
  0.0 31.2 jit_solution(15723595121158820174)
XLA Ops:
  0.0 30.5 %shard_map.91 = bf16[256,512]{1,0:T(8,128)(2,1)S(1)} custom-call(bf16[256,2048]{1,0:T(8,128)(2,1)} %tok_hbm.1, bf16[1,2048,1024]{2,1,0:T(8,128)(2,1)} %gate_hbm.1, bf16[1,2048,1024]{2,1,0:T(8,128)(2,1)} %up_hbm.1, bf16[1,1024,2048]{2,1,0:T(8,128)(2,1)} %down_hbm.1, bf16[2048,256]{1,0:T(8,128)(2,1)} %side_hbm.1, bf16[1024,512]{1,0:T(8,128)(2,1)} %dout_hbm.1, ...), custom_call_target="tpu_custom_call" | custom-call | tf_op jit(solution)/shard_map/pallas_call | solution.py:480
  30.5 0.7 %copy.11 = bf16[256,512]{1,0:T(8,128)(2,1)} copy(bf16[256,512]{1,0:T(8,128)(2,1)S(1)} %shard_map.91) | data formatting | bytes 524288
